TPU v7x, 32 devices: a whole 2x2x4 slice. The times are simulated.
32 devices in a mesh: sp: 8 (over z, x), dp: 4 (over y, core).
Axes of the slice: x: 2, y: 2, z: 4, core: 2. Of those that a mesh axis runs over, the one named last changes fastest.
Arguments:
- normed_input: bfloat16 [2560, 2048], P('sp'), may hold values from -6 to 6
- out_grad: bfloat16 [2560, 2048], P('sp'), may hold values from -6 to 6
- value_weight: bfloat16 [2048, 1024], P(None, 'dp'), may hold values from -0.125 to 0.125
- gate_weight: bfloat16 [2048, 1024], P(None, 'dp'), may hold values from -0.125 to 0.125
- down_weight: bfloat16 [1024, 2048], P('dp'), may hold values from -0.1875 to 0.1875
- conv_kernel: float32 [31, 1024], P(None, 'dp'), may hold values from -5 to 5
- conv_bias: float32 [1024], P('dp'), may hold values from -3 to 3
- norm_gain: float32 [1024], P('dp'), may hold values from 0.1 to 1.9
- norm_shift: float32 [1024], P('dp'), may hold values from -3 to 3
Outputs:
- input_grad: bfloat16 [2560, 2048], P('sp')
- value_grad: float32 [2048, 1024], P('sp', 'dp')
- gate_grad: float32 [2048, 1024], P('sp', 'dp')
- down_grad: float32 [1024, 2048], P('dp', 'sp')
- kernel_grad: float32 [31, 1024], P(None, 'dp')
- bias_grad: float32 [1024], P('dp')
- gain_grad: float32 [1024], P('dp')
- shift_grad: float32 [1024], P('dp')
All inputs are finite; a program needn't handle non-finite values.
Results may differ from a plain program's by a relative error of at most 0.006.
Values may be sent and summed in bfloat16 or wider, within the bound.
No kernel may reach another device: no remote copies, remote signals or barrier semaphores. Data moves between devices by JAX's collectives and lax.ppermute only.
A program may use at most 64 MiB of HBM per device.

v0:
```python
import math

import jax
import jax.numpy as jnp
from jax import lax
from jax.sharding import PartitionSpec as P

EPS = 1e-05


def with_halo(block, sides, width):
    for axis, dim in sides:
        count = lax.axis_size(axis)
        forward = [(i, i + 1) for i in range(count - 1)]
        backward = [(target, source) for source, target in forward]
        low = lax.ppermute(
            lax.slice_in_dim(block, block.shape[dim] - width, None, axis=dim), axis, forward
        )
        high = lax.ppermute(lax.slice_in_dim(block, 0, width, axis=dim), axis, backward)
        block = jnp.concatenate([low, block, high], axis=dim)
    return block


def project(weight, rows):
    return lax.dot_general(
        weight, rows, (((0,), (1,)), ((), ())), preferred_element_type=jnp.float32
    )


def on_device(
    normed_input,
    out_grad,
    value_weight,
    gate_weight,
    down_weight,
    conv_kernel,
    conv_bias,
    norm_gain,
    norm_shift,
):
    tokens = normed_input.shape[0]
    width = conv_kernel.shape[0]
    reach = width // 2
    local_channels = value_weight.shape[1]
    channels = local_channels * lax.axis_size("dp")
    ratio = 1.0 / math.sqrt(tokens * lax.axis_size("sp"))
    value_b = project(value_weight, normed_input).astype(jnp.bfloat16)
    gate_b = project(gate_weight, normed_input).astype(jnp.bfloat16)
    value = lax.optimization_barrier(value_b).astype(jnp.float32)
    gate = lax.optimization_barrier(gate_b).astype(jnp.float32)
    opening = jax.nn.sigmoid(gate)
    glu = value * opening
    padded = with_halo(glu, (("sp", 1),), reach)
    mixed = jnp.zeros_like(glu) + conv_bias[:, None]
    for tap in range(width):
        mixed = mixed + conv_kernel[tap][:, None] * padded[:, tap : tap + tokens]
    total, squares = lax.psum((jnp.sum(mixed, axis=0), jnp.sum(mixed * mixed, axis=0)), "dp")
    mean = total / channels
    spread = squares / channels - mean * mean
    inv_std = lax.rsqrt(spread + EPS)
    centred = (mixed - mean[None, :]) * inv_std[None, :]
    normed = centred * norm_gain[:, None] + norm_shift[:, None]
    sig = jax.nn.sigmoid(normed)
    activated = (normed * sig).astype(jnp.bfloat16)
    d_act = lax.dot_general(
        down_weight, out_grad, (((1,), (1,)), ((), ())), preferred_element_type=jnp.float32
    )
    d_normed = d_act * sig * (1.0 + normed * (1.0 - sig))
    d_centred = d_normed * norm_gain[:, None]
    first, second = lax.psum(
        (jnp.sum(d_centred, axis=0), jnp.sum(d_centred * centred, axis=0)), "dp"
    )
    d_mixed = inv_std[None, :] * (
        d_centred - first[None, :] / channels - centred * (second[None, :] / channels)
    )
    d_padded = with_halo(d_mixed, (("sp", 1),), reach)
    d_glu = jnp.zeros_like(d_mixed)
    for tap in range(width):
        d_glu = (
            d_glu
            + conv_kernel[tap][:, None] * d_padded[:, 2 * reach - tap : 2 * reach - tap + tokens]
        )
    kernel_local = jnp.stack(
        [jnp.sum(d_mixed * padded[:, tap : tap + tokens], axis=1) for tap in range(width)]
    )
    kernel_grad, bias_grad, gain_grad, shift_grad = lax.psum(
        (
            kernel_local * ratio,
            jnp.sum(d_mixed, axis=1) * ratio,
            jnp.sum(d_normed * centred, axis=1) * ratio,
            jnp.sum(d_normed, axis=1) * ratio,
        ),
        "sp",
    )
    d_value = (d_glu * opening).astype(jnp.bfloat16)
    d_gate = (d_glu * value * opening * (1.0 - opening)).astype(jnp.bfloat16)
    numbers = (((0,), (1,)), ((), ()))
    value_part = lax.dot_general(normed_input, d_value, numbers, preferred_element_type=jnp.float32)
    gate_part = lax.dot_general(normed_input, d_gate, numbers, preferred_element_type=jnp.float32)
    down_part = lax.dot_general(out_grad, activated, numbers, preferred_element_type=jnp.float32)
    summed = lax.psum_scatter(
        jnp.concatenate([value_part, gate_part, down_part], axis=1) * ratio,
        "sp",
        scatter_dimension=0,
        tiled=True,
    )
    value_grad = summed[:, :local_channels]
    gate_grad = summed[:, local_channels : 2 * local_channels]
    down_grad = summed[:, 2 * local_channels :].T
    numbers = (((0,), (1,)), ((), ()))
    own = lax.dot_general(d_value, value_weight, numbers, preferred_element_type=jnp.float32)
    own = own + lax.dot_general(d_gate, gate_weight, numbers, preferred_element_type=jnp.float32)
    input_grad = lax.psum(own, "dp").astype(jnp.bfloat16)
    return (
        input_grad,
        value_grad,
        gate_grad,
        down_grad,
        kernel_grad,
        bias_grad,
        gain_grad,
        shift_grad,
    )


def solution(mesh):
    in_specs = (
        P("sp", None),
        P("sp", None),
        P(None, "dp"),
        P(None, "dp"),
        P("dp", None),
        P(None, "dp"),
        P("dp"),
        P("dp"),
        P("dp"),
    )
    out_specs = (
        P("sp", None),
        P("sp", "dp"),
        P("sp", "dp"),
        P("dp", "sp"),
        P(None, "dp"),
        P("dp"),
        P("dp"),
        P("dp"),
    )
    return jax.shard_map(
        on_device, mesh=mesh, in_specs=in_specs, out_specs=out_specs, check_vma=False
    )
```

profile of v0, /device:TPU:0, one launch (start us, length us, event | category | flops | bytes accessed | tf_op | source)
XLA Modules:
  0.0 185.2 jit_solution(6150821379646648669)
XLA Ops:
  7.2 0.0 copy-start
  7.2 0.0 copy-start.1
  7.2 0.0 reduce-scatter.2.cloned.1.call-start
  7.2 1.2 copy-done
  8.5 1.7 convolution_convert_fusion.1
  10.2 0.0 copy-done.1
  10.2 0.0 copy-start.3
  10.2 0.0 copy-start.5
  10.3 0.0 copy-start.4
  10.3 0.0 copy-start.6
  10.3 0.5 convolution_convert_fusion
  10.8 0.1 convert_multiply_fusion.1
  10.9 4.9 %collective-permute-start = (f32[256,15]{0,1:T(8,128)S(1)}, f32[256,15]{0,1:T(8,128)S(1)}, u32[]{:S(2)}, u32[]{:S(2)}) collective-permute-start(f32[256,15]{0,1:T(8,128)S(1)} %get-tuple-element.71), channel_id=1, source_target_pairs={{0,4},{4,8},{8,12},{12,16},{16,20},{20,24},{24,28},{1,5},{5,9},{9,... | collective-permute-start | bytes 46088 | tf_op jit(solution)/shard_map/ppermute | solution.py:16
  15.8 1.3 collective-permute-start.1
  17.1 0.0 copy-done.3
  17.2 0.1 collective-permute-done
  17.2 4.2 %collective-permute-done.1 = f32[256,15]{0,1:T(8,128)S(1)} collective-permute-done((f32[256,15]{0,1:T(8,128)S(1)}, f32[256,15]{0,1:T(8,128)S(1)}, u32[]{:S(2)}, u32[]{:S(2)}) %collective-permute-start.1) | collective-permute-done | bytes 15392 | tf_op jit(solution)/shard_map/ppermute | solution.py:19
  21.4 0.0 copy-done.5
  21.4 1.7 multiply_reduce_fusion.33
  23.2 5.7 %all-reduce.2 = (f32[320]{0:T(512)S(1)}, f32[320]{0:T(512)S(1)}) all-reduce(f32[320]{0:T(512)S(1)} %get-tuple-element.53, f32[320]{0:T(512)S(1)} %get-tuple-element.52), channel_id=1, replica_groups=mesh['sp'=8,'dp'=4] {'dp'}, use_global_device_ids=true, to_apply=%region_3.0 | all-reduce | flops 640 | bytes 5120 | tf_op jit(solution)/shard_map/psum | solution.py:57
  28.8 0.0 copy-done.4
  28.8 0.0 copy-done.6
  28.8 2.4 %multiply_reduce_fusion = (f32[256]{0:T(256)S(1)}, f32[320]{0:T(512)S(1)}, f32[320]{0:T(512)S(1)}, f32[256]{0:T(256)S(1)}, f32[256,320]{0,1:T(8,128)S(1)}) fusion(f32[256,320]{0,1:T(8,128)S(1)} %get-tuple-element.65, f32[320]{0:T(512)S(1)} %get-tuple-element.105, f32[320]{0:T(512)S(1)} %get-tuple-element.104, f32[256]{0:T(256)S(1)} %copy-done.4, ...), kind=kOutput, calls=%fused_computation.214 | convolution fusion | flops 337099648 | bytes 3023872 | tf_op jit(solution)/shard_map/dot_general | solution.py:65
  31.2 6.6 %all-reduce.1 = (f32[320]{0:T(512)S(1)}, f32[320]{0:T(512)S(1)}) all-reduce(f32[320]{0:T(512)S(1)} %get-tuple-element.47, f32[320]{0:T(512)S(1)} %get-tuple-element.48), channel_id=1, replica_groups=mesh['sp'=8,'dp'=4] {'dp'}, use_global_device_ids=true, to_apply=%region_7.0 | all-reduce | flops 640 | bytes 5120 | tf_op jit(solution)/shard_map/psum | solution.py:70
  37.9 0.5 multiply_reduce_fusion.1
  38.4 1.3 collective-permute-start.2
  39.7 5.0 %collective-permute-start.3 = (f32[256,15]{0,1:T(8,128)S(1)}, f32[256,15]{0,1:T(8,128)S(1)}, u32[]{:S(2)}, u32[]{:S(2)}) collective-permute-start(f32[256,15]{0,1:T(8,128)S(1)} %get-tuple-element.70), channel_id=1, source_target_pairs={{0,4},{4,8},{8,12},{12,16},{16,20},{20,24},{24,28},{1,5},{5,9},{9,... | collective-permute-start | bytes 46088 | tf_op jit(solution)/shard_map/ppermute | solution.py:16
  44.7 2.2 %convolution_bitcast_fusion = f32[2048,256]{0,1:T(8,128)S(1)} fusion(bf16[320,2048]{1,0:T(8,128)(2,1)} %param.10, f32[256,320]{0,1:T(8,128)S(1)} %get-tuple-element.65, f32[256]{0:T(256)S(1)} %copy-done.6, f32[256]{0:T(256)S(1)} %copy-done.4, f32[320]{0:T(512)S(1)} %get-tuple-element.105, f32[320]{0:T(512)S(1)} %get-tuple-element.104), kind=kOutput, calls=%fused_computation.2 | convolution fusion | flops 336281600 | bytes 3740160 | tf_op jit(solution)/shard_map/dot_general | solution.py:100
  46.9 0.0 collective-permute-done.2
  46.9 0.0 collective-permute-done.3
  46.9 1.7 fusion.3
  48.6 0.7 convolution_bitcast_fusion.1
  49.3 0.8 convolution_bitcast_fusion.2
  50.1 3.3 %maximum_multiply_fusion = f32[2048,768]{0,1:T(8,128)} fusion(f32[2048,256]{0,1:T(8,128)S(1)} %convolution_bitcast_fusion, f32[2048,256]{0,1:T(8,128)S(1)} %convolution_bitcast_fusion.1, f32[2048,256]{0,1:T(8,128)S(1)} %convolution_bitcast_fusion.2), kind=kLoop, calls=%fused_computation | loop fusion | flops 4718592 | bytes 12582912 | tf_op jit(solution)/shard_map/mul | solution.py:102
  53.4 0.0 reduce-scatter.2.cloned.1.call-update
  53.4 0.3 multiply_reduce_fusion.26
  53.7 0.4 multiply_reduce_fusion.17
  54.1 0.4 multiply_reduce_fusion.10
  54.5 0.1 stack.127
  54.6 0.0 copy-start.2
  54.6 40.4 %all-reduce = (f32[31,256]{1,0:T(8,128)}, f32[256]{0:T(256)}, f32[256]{0:T(256)}, f32[256]{0:T(256)}) all-reduce(f32[31,256]{1,0:T(8,128)S(1)} %broadcast_multiply_fusion, f32[256]{0:T(256)S(1)} %broadcast_multiply_fusion.6, f32[256]{0:T(256)S(1)} %get-tuple-element.108, ...), channel_id=1, replica_groups=mesh['sp'=8,'dp'=4] {'sp'}, use_global_device_ids=true, to_apply=%region_41.0 | all-reduce | flops 8704 | bytes 69632 | tf_op jit(solution)/shard_map/psum | solution.py:86
  95.0 1.8 fusion.126
  96.8 2.1 %convolution_add_fusion = f32[320,2048]{1,0:T(8,128)} fusion(f32[320,2048]{1,0:T(8,128)S(1)} %fusion.126, bf16[256,320]{0,1:T(8,128)(2,1)S(1)} %get-tuple-element.63, bf16[2048,256]{1,0:T(8,128)(2,1)S(1)} %copy-done.2), kind=kOutput, calls=%fused_computation.1 | convolution fusion | flops 336199680 | bytes 6455296 | tf_op jit(solution)/shard_map/dot_general | solution.py:112
  98.9 50.2 %all-reduce.4 = bf16[320,2048]{1,0:T(8,128)(2,1)} all-reduce(f32[320,2048]{1,0:T(8,128)} %convolution_add_fusion), channel_id=1, replica_groups=mesh['sp'=8,'dp'=4] {'dp'}, use_global_device_ids=true, to_apply=%region_8.0 | all-reduce | flops 655360 | bytes 3932160 | tf_op jit(solution)/shard_map/psum | solution.py:113
  149.1 25.7 %reduce-scatter.2.cloned.1.call-done = f32[256,768]{0,1:T(8,128)} async-done(((f32[2048,768]{0,1:T(8,128)}), f32[256,768]{0,1:T(8,128)}) %reduce-scatter.2.cloned.1.call-update) | async-done | bytes 786448 | tf_op jit(solution)/shard_map/reduce_scatter | solution.py:101
  174.8 1.9 %slice_bitcast_fusion = (f32[256,256]{1,0:T(8,128)}, f32[256,256]{0,1:T(8,128)S(1)}, f32[256,256]{0,1:T(8,128)S(1)}) fusion(f32[256,768]{0,1:T(8,128)} %reduce-scatter.2.cloned.1.call-done), kind=kLoop, calls=%fused_computation.257 | loop fusion | bytes 1572864 | tf_op jit(solution)/shard_map/transpose | solution.py:109
  176.6 0.8 copy.18
  177.5 0.8 copy.17
  (10 shorter events, 0.1 us)
Async XLA Ops:
  7.2 1.3 copy-start
  7.2 3.0 %copy-start.1 = (bf16[2048,256]{1,0:T(8,128)(2,1)S(1)}, bf16[2048,256]{1,0:T(8,128)(2,1)}, u32[]{:S(2)}) copy-start(bf16[2048,256]{1,0:T(8,128)(2,1)} %param.12) | copy-start | bytes 3145732
  7.2 167.6 %reduce-scatter.2.cloned.1.call-start = ((), (), s32[]{:S(2)}) async-start(), calls=%async_computation.1 | async-start | bytes 7077888 | tf_op jit(solution)/shard_map/reduce_scatter | solution.py:101
  10.2 6.9 %copy-start.3 = (f32[31,256]{1,0:T(8,128)S(1)}, f32[31,256]{1,0:T(8,128)}, u32[]{:S(2)}) copy-start(f32[31,256]{1,0:T(8,128)} %param.14) | copy-start | bytes 95236
  10.2 11.2 %copy-start.5 = (f32[256]{0:T(256)S(1)}, f32[256]{0:T(256)}, u32[]{:S(2)}) copy-start(f32[256]{0:T(256)} %param.15) | copy-start | bytes 3076
  10.3 18.6 %copy-start.4 = (f32[256]{0:T(256)S(1)}, f32[256]{0:T(256)}, u32[]{:S(2)}) copy-start(f32[256]{0:T(256)} %param.16) | copy-start | bytes 3076
  10.3 18.6 %copy-start.6 = (f32[256]{0:T(256)S(1)}, f32[256]{0:T(256)}, u32[]{:S(2)}) copy-start(f32[256]{0:T(256)} %param.17) | copy-start | bytes 3076
  10.9 6.3 %collective-permute-start = (f32[256,15]{0,1:T(8,128)S(1)}, f32[256,15]{0,1:T(8,128)S(1)}, u32[]{:S(2)}, u32[]{:S(2)}) collective-permute-start(f32[256,15]{0,1:T(8,128)S(1)} %get-tuple-element.71), channel_id=1, source_target_pairs={{0,4},{4,8},{8,12},{12,16},{16,20},{20,24},{24,28},{1,5},{5,9},{9,... | collective-permute-start | bytes 46088 | tf_op jit(solution)/shard_map/ppermute | solution.py:16
  15.8 5.6 %collective-permute-start.1 = (f32[256,15]{0,1:T(8,128)S(1)}, f32[256,15]{0,1:T(8,128)S(1)}, u32[]{:S(2)}, u32[]{:S(2)}) collective-permute-start(f32[256,15]{0,1:T(8,128)S(1)} %get-tuple-element.72), channel_id=1, source_target_pairs={{4,0},{8,4},{12,8},{16,12},{20,16},{24,20},{28,24},{5,1},{9,5},{13... | collective-permute-start | bytes 46088 | tf_op jit(solution)/shard_map/ppermute | solution.py:19
  38.4 8.5 %collective-permute-start.2 = (f32[256,15]{0,1:T(8,128)S(1)}, f32[256,15]{0,1:T(8,128)S(1)}, u32[]{:S(2)}, u32[]{:S(2)}) collective-permute-start(f32[256,15]{0,1:T(8,128)S(1)} %get-tuple-element.69), channel_id=1, source_target_pairs={{4,0},{8,4},{12,8},{16,12},{20,16},{24,20},{28,24},{5,1},{9,5},{13... | collective-permute-start | bytes 46088 | tf_op jit(solution)/shard_map/ppermute | solution.py:19
  39.7 7.2 %collective-permute-start.3 = (f32[256,15]{0,1:T(8,128)S(1)}, f32[256,15]{0,1:T(8,128)S(1)}, u32[]{:S(2)}, u32[]{:S(2)}) collective-permute-start(f32[256,15]{0,1:T(8,128)S(1)} %get-tuple-element.70), channel_id=1, source_target_pairs={{0,4},{4,8},{8,12},{12,16},{16,20},{20,24},{24,28},{1,5},{5,9},{9,... | collective-permute-start | bytes 46088 | tf_op jit(solution)/shard_map/ppermute | solution.py:16
  54.6 42.2 %copy-start.2 = (bf16[2048,256]{1,0:T(8,128)(2,1)S(1)}, bf16[2048,256]{1,0:T(8,128)(2,1)}, u32[]{:S(2)}) copy-start(bf16[2048,256]{1,0:T(8,128)(2,1)} %param.12) | copy-start | bytes 3145732
Sparse Core Ops, SparseCore 0:
  53.5 121.1 reduce-scatter.1
where the time goes:
time: 186 us; the launch traced here: 185 us
  blocking collectives  103 us (55%)
  waiting for transfers between devices  30 us (16%)
  between operations  14.3 us (8%)
  starting transfers between devices  12.5 us (7%)
  matrix products  12.2 us (7%)
  other arithmetic  8.41 us (5%)
  local copies, waits for them, and re-layouts  4.97 us (3%)
    psum x1, blocking collectives, on_device(): input_grad = lax.psum(own, 'dp').astype(jnp.bfloat16)  50.2 us
    psum x1, blocking collectives, on_device(): lax.psum((kernel_local * ratio, jnp.sum(d_mixed, axis=1) * ratio, jnp.sum...  40.4 us
    reduce_scatter x1, waiting for transfers between devices, on_device(): lax.psum_scatter(jnp.concatenate([value_part, gate_part, down_part], axis...  25.7 us
    ppermute x2, starting transfers between devices, with_halo(): lax.ppermute(lax.slice_in_dim(block, block.shape[dim] - width, None, axis...  9.85 us
    psum x1, blocking collectives, on_device(): lax.psum((jnp.sum(d_centred, axis=0), jnp.sum(d_centred * centred, axis=0...  6.65 us
    psum x1, blocking collectives, on_device(): lax.psum((jnp.sum(mixed, axis=0), jnp.sum(mixed * mixed, axis=0)), 'dp')  5.67 us
    ppermute x2, waiting for transfers between devices, with_halo(): lax.ppermute(lax.slice_in_dim(block, 0, width, axis=dim), axis, backward)  4.21 us
  transfers between devices with their start and end apart: 5, of which 3 were waited for; matrix products, arithmetic and copies ran while one was open for 4% of the time, Pallas kernels for 0%

commit v1 on v0

v1 whole, which is shorter than its diff:
```python
import math

import jax
import jax.numpy as jnp
from jax import lax
from jax.sharding import PartitionSpec as P


EPS = 1e-05


def dot(a, b, ca, cb):
    return lax.dot_general(a, b, (((ca,), (cb,)), ((), ())), preferred_element_type=jnp.float32)


def butterfly(array, axis):
    count = lax.axis_size(axis)
    bit = count // 2
    while bit:
        arrived = lax.ppermute(array, axis, [(i, i ^ bit) for i in range(count)])
        array = array + arrived
        bit //= 2
    return array


def columns_of(rows, parity):
    count = lax.axis_size("sp")
    block = rows.shape[1] // count
    return jnp.concatenate(
        [
            lax.dynamic_slice_in_dim(rows, (2 * j + parity) * block, block, axis=1)
            for j in range(count // 2)
        ],
        axis=1,
    )


def send_pair(part, ratio):
    count = lax.axis_size("sp")
    part = (part * ratio).astype(jnp.bfloat16)
    return part, lax.ppermute(part, "sp", [(i, i ^ 1) for i in range(count)])


def finish_scatter(part, got, ratio, axis):
    count = lax.axis_size("sp")
    groups = count // 2
    place = lax.axis_index("sp") // 2
    pair = part * ratio + got.astype(jnp.float32)
    block = pair.shape[axis] // groups

    def piece(which):
        return lax.dynamic_slice_in_dim(pair, which * block, block, axis=axis)

    out = piece(place)
    sent = []
    for step in range(1, groups):
        send = piece((place + step) % groups).astype(jnp.bfloat16)
        targets = [(i, ((i // 2 + step) % groups) * 2 + i % 2) for i in range(count)]
        arrived = lax.ppermute(send, "sp", targets)
        sent.append(send)
        out = out + arrived.astype(jnp.float32)
    return out, sent


def halves(own):
    side = lax.axis_index("dp") % 2
    half = own.shape[1] // 2
    keep = lax.dynamic_slice_in_dim(own, side * half, half, axis=1)
    give = lax.dynamic_slice_in_dim(own, (1 - side) * half, half, axis=1)
    return keep, give.astype(jnp.bfloat16)


def sum_over_dp(keep, give):
    count = lax.axis_size("dp")
    side = lax.axis_index("dp") % 2
    pairs = [(i, i ^ 1) for i in range(count)]
    arrived = lax.ppermute(give, "dp", pairs)
    part = keep + arrived.astype(jnp.float32)
    bit = 2
    while bit < count:
        part = part.astype(jnp.bfloat16)
        arrived = lax.ppermute(part, "dp", [(i, i ^ bit) for i in range(count)])
        part = part.astype(jnp.float32) + arrived.astype(jnp.float32)
        bit *= 2
    part = part.astype(jnp.bfloat16)
    arrived = lax.ppermute(part, "dp", pairs)
    first = jnp.where(side == 0, part, arrived)
    second = jnp.where(side == 0, arrived, part)
    return jnp.concatenate([first, second], axis=1)


def on_device(
    normed_input,
    out_grad,
    value_weight,
    gate_weight,
    down_weight,
    conv_kernel,
    conv_bias,
    norm_gain,
    norm_shift,
):
    tokens = normed_input.shape[0]
    width = conv_kernel.shape[0]
    reach = width // 2
    wide = tokens + 2 * reach
    channels = value_weight.shape[1] * lax.axis_size("dp")
    ratio = 1.0 / math.sqrt(tokens * lax.axis_size("sp"))

    value_b = dot(normed_input, value_weight, 1, 0).astype(jnp.bfloat16)
    gate_b = dot(normed_input, gate_weight, 1, 0).astype(jnp.bfloat16)
    value = lax.optimization_barrier(value_b).astype(jnp.float32)
    gate = lax.optimization_barrier(gate_b).astype(jnp.float32)
    opening = jax.nn.sigmoid(gate)
    glu = value * opening
    act_main = dot(out_grad, down_weight, 1, 1)
    forward = [(i, i + 1) for i in range(lax.axis_size("sp") - 1)]
    backward = [(target, source) for source, target in forward]
    low = jnp.concatenate([glu[tokens - 2 * reach :], act_main[tokens - reach :]], axis=0)
    high = jnp.concatenate([glu[: 2 * reach], act_main[:reach]], axis=0)
    low = lax.ppermute(low, "sp", forward)
    high = lax.ppermute(high, "sp", backward)
    glu_low, glu_high = low[: 2 * reach], high[: 2 * reach]
    padded = jnp.concatenate([glu_low, glu, glu_high], axis=0)
    mixed = jnp.zeros((wide, glu.shape[1]), jnp.float32) + conv_bias[None, :]
    for tap in range(width):
        mixed = mixed + conv_kernel[tap][None, :] * padded[tap : tap + wide]
    total, squares = lax.psum((jnp.sum(mixed, axis=1), jnp.sum(mixed * mixed, axis=1)), "dp")
    d_act = jnp.concatenate([low[2 * reach :], act_main, high[2 * reach :]], axis=0)
    mean = total / channels
    spread = jnp.maximum(squares / channels - mean * mean, 0.0)
    inv_std = lax.rsqrt(spread + EPS)
    centred = (mixed - mean[:, None]) * inv_std[:, None]
    normed = centred * norm_gain[None, :] + norm_shift[None, :]
    sig = jax.nn.sigmoid(normed)
    d_normed = d_act * sig * (1.0 + normed * (1.0 - sig))
    d_centred = d_normed * norm_gain[None, :]
    here = slice(reach, reach + tokens)
    activated = (normed * sig)[here].astype(jnp.bfloat16)
    parity = lax.axis_index("sp") % 2
    sums = (jnp.sum(d_centred, axis=1), jnp.sum(d_centred * centred, axis=1))
    down_sent, down_got = send_pair(dot(activated, columns_of(out_grad, 1 - parity), 0, 0), ratio)
    sums, _ = lax.optimization_barrier((sums, down_sent))
    first, second = lax.psum(sums, "dp")
    d_mixed = inv_std[:, None] * (
        d_centred - first[:, None] / channels - centred * (second[:, None] / channels)
    )
    d_glu = jnp.zeros_like(glu)
    for tap in range(width):
        start = 2 * reach - tap
        d_glu = d_glu + conv_kernel[tap][None, :] * d_mixed[start : start + tokens]
    d_value = (d_glu * opening).astype(jnp.bfloat16)
    d_gate = (d_glu * value * opening * (1.0 - opening)).astype(jnp.bfloat16)
    input_other = columns_of(normed_input, 1 - parity)
    value_sent, value_got = send_pair(dot(input_other, d_value, 0, 0), ratio)
    gate_sent, gate_got = send_pair(dot(input_other, d_gate, 0, 0), ratio)
    d_value, d_gate, _, _ = lax.optimization_barrier((d_value, d_gate, value_sent, gate_sent))
    own = dot(d_value, value_weight, 1, 1) + dot(d_gate, gate_weight, 1, 1)
    keep, give = halves(own)
    input_grad = sum_over_dp(keep, give)
    grad_late, activated, _ = lax.optimization_barrier((out_grad, activated, give))
    grad_own = columns_of(grad_late, parity)
    down_grad, down_sent = finish_scatter(dot(activated, grad_own, 0, 0), down_got, ratio, 1)
    input_late, d_mixed, d_normed, _ = lax.optimization_barrier(
        (normed_input, d_mixed, d_normed, down_sent)
    )
    input_own = columns_of(input_late, parity)
    value_grad, _ = finish_scatter(dot(input_own, d_value, 0, 0), value_got, ratio, 0)
    gate_grad, _ = finish_scatter(dot(input_own, d_gate, 0, 0), gate_got, ratio, 0)
    d_here = d_mixed[here]
    sums = [
        jnp.sum(d_here * padded[reach + tap : reach + tap + tokens], axis=0)
        for tap in range(width)
    ]
    sums.append(jnp.sum(d_here, axis=0))
    sums.append(jnp.sum((d_normed * centred)[here], axis=0))
    sums.append(jnp.sum(d_normed[here], axis=0))
    small = butterfly(jnp.stack(sums) * ratio, "sp")
    return (
        input_grad,
        value_grad,
        gate_grad,
        down_grad,
        small[:width],
        small[width],
        small[width + 1],
        small[width + 2],
    )


def solution(mesh):
    in_specs = (
        P("sp", None),
        P("sp", None),
        P(None, "dp"),
        P(None, "dp"),
        P("dp", None),
        P(None, "dp"),
        P("dp"),
        P("dp"),
        P("dp"),
    )
    out_specs = (
        P("sp", None),
        P("sp", "dp"),
        P("sp", "dp"),
        P("dp", "sp"),
        P(None, "dp"),
        P("dp"),
        P("dp"),
        P("dp"),
    )

    return jax.shard_map(
        on_device, mesh=mesh, in_specs=in_specs, out_specs=out_specs, check_vma=False
    )
```

time: 186 us -> 114 us (0.61)
  blocking collectives: 103 us -> 13 us
  starting transfers between devices: 12.5 us -> 29.3 us
  between operations: 14.3 us -> 1.8 us
  other arithmetic: 8.41 us -> 15.4 us
  local copies, waits for them, and re-layouts: 4.97 us -> 10.6 us
    psum x4 -> x2, blocking collectives: 103 us -> 13 us  [the longest x1 6.57 us: on_device(): lax.psum((jnp.sum(mixed, axis=1), jnp.sum(mixed * mixed, axis=1)), 'dp')]
    ppermute x4 -> x20, waiting for transfers between devices: 4.28 us -> 31.5 us  [the longest x9 16.1 us: finish_scatter(): arrived = lax.ppermute(send, 'sp', targets)]
    reduce_scatter x1 -> x0, waiting for transfers between devices: 25.7 us -> none  [on_device(): lax.psum_scatter(jnp.concatenate([value_part, gate_part, down_part], axis...]
    ppermute x4 -> x20, starting transfers between devices: 12.4 us -> 29.3 us  [the longest x9 12.1 us: finish_scatter(): arrived = lax.ppermute(send, 'sp', targets)]
    add x0 -> x6, other arithmetic: none -> 4.3 us  [the longest x3 4.28 us: finish_scatter(): out = out + arrived.astype(jnp.float32)]
    convert_element_type x0 -> x4, local copies, waits for them, and re-layouts: none -> 2.52 us  [the longest x3 1.58 us: finish_scatter(): send = piece((place + step) % groups).astype(jnp.bfloat16)]
    dynamic_slice x0 -> x3, local copies, waits for them, and re-layouts: none -> 2.4 us  [columns_of(): lax.dynamic_slice_in_dim(rows, (2 * j + parity) * block, block, axis=1)]
    mul x4 -> x2, other arithmetic: 3.29 us -> 0.89 us  [the longest x1 0.88 us: on_device(): inv_std[:, None]]
  transfers between devices with their start and end apart: 5 -> 20, of which waited for: 3 -> 9; matrix products, arithmetic and copies ran while one was open for 4% -> 22% of each run, Pallas kernels for 0% -> 0%
where the time goes in v1:
time: 114 us; the launch traced here: 113 us
  waiting for transfers between devices  31.5 us (28%)
  starting transfers between devices  29.3 us (26%)
  other arithmetic  15.4 us (14%)
  blocking collectives  13 us (11%)
  matrix products  11.7 us (10%)
  local copies, waits for them, and re-layouts  10.6 us (9%)
  between operations  1.8 us (2%)
    ppermute x9, waiting for transfers between devices, finish_scatter(): arrived = lax.ppermute(send, 'sp', targets)  16.1 us
    ppermute x9, starting transfers between devices, finish_scatter(): arrived = lax.ppermute(send, 'sp', targets)  12.1 us
    dot_general x11, matrix products, dot(): lax.dot_general(a, b, (((ca,), (cb,)), ((), ())), preferred_element_type=...  11.7 us
    ppermute x3, waiting for transfers between devices, butterfly(): arrived = lax.ppermute(array, axis, [(i, i ^ bit) for i in range(count)])  7.72 us
    psum x1, blocking collectives, on_device(): lax.psum((jnp.sum(mixed, axis=1), jnp.sum(mixed * mixed, axis=1)), 'dp')  6.57 us
    psum x1, blocking collectives, on_device(): first, second = lax.psum(sums, 'dp')  6.38 us
    ppermute x1, starting transfers between devices, on_device(): low = lax.ppermute(low, 'sp', forward)  5.5 us
    ppermute x3, starting transfers between devices, butterfly(): arrived = lax.ppermute(array, axis, [(i, i ^ bit) for i in range(count)])  4.41 us
  transfers between devices with their start and end apart: 20, of which 9 were waited for; matrix products, arithmetic and copies ran while one was open for 22% of the time, Pallas kernels for 0%

profile of v1, /device:TPU:0, one launch (start us, length us, event | category | flops | bytes accessed | tf_op | source)
XLA Modules:
  0.0 113.3 jit_solution(10748869048840716451)
XLA Ops:
  0.7 1.2 %copy-done = bf16[2048,256]{1,0:T(8,128)(2,1)S(1)} copy-done((bf16[2048,256]{1,0:T(8,128)(2,1)S(1)}, bf16[2048,256]{1,0:T(8,128)(2,1)}, u32[]{:S(2)}) %copy-start) | copy-done | bytes 1048600
  1.9 1.8 %convolution_convert_fusion.1 = bf16[320,256]{1,0:T(8,128)(2,1)S(1)} fusion(bf16[320,2048]{1,0:T(8,128)(2,1)} %param.9, bf16[2048,256]{1,0:T(8,128)(2,1)S(1)} %copy-done), kind=kOutput, calls=%fused_computation.47 | convolution fusion | flops 335626240 | bytes 2523136 | tf_op jit(solution)/shard_map/dot_general | solution.py:13
  4.3 0.8 copy-done.2
  5.4 0.5 fusion.193
  6.7 1.3 %collective-permute-start.1 = (f32[45,256]{1,0:T(8,128)S(1)}, f32[45,256]{1,0:T(8,128)S(1)}, u32[]{:S(2)}, u32[]{:S(2)}) collective-permute-start(f32[45,256]{1,0:T(8,128)S(1)} %pad_maximum_fusion.11), channel_id=1, source_target_pairs={{4,0},{8,4},{12,8},{16,12},{20,16},{24,20},{28,24},{5,1},{9,5},{13... | collective-permute-start | bytes 138248 | tf_op jit(solution)/shard_map/ppermute | solution.py:122
  8.0 5.5 %collective-permute-start = (f32[45,256]{1,0:T(8,128)S(1)}, f32[45,256]{1,0:T(8,128)S(1)}, u32[]{:S(2)}, u32[]{:S(2)}) collective-permute-start(f32[45,256]{1,0:T(8,128)S(1)} %pad_maximum_fusion.10), channel_id=1, source_target_pairs={{0,4},{4,8},{8,12},{12,16},{16,20},{20,24},{24,28},{1,5},{5,9},{9,... | collective-permute-start | bytes 138248 | tf_op jit(solution)/shard_map/ppermute | solution.py:121
  13.9 2.2 %constant_dynamic-slice_fusion.11 = (bf16[320,256]{1,0:T(8,128)(2,1)}, bf16[320,256]{1,0:T(8,128)(2,1)}, bf16[320,256]{1,0:T(8,128)(2,1)}, bf16[320,256]{1,0:T(8...) fusion(bf16[320,2048]{1,0:T(8,128)(2,1)} %param.9, ...), kind=kLoop, calls=%fused_computation.331 | loop fusion | bytes 2621456 | tf_op jit(solution)/shard_map/dynamic_slice | solution.py:31
  16.4 1.6 %multiply_reduce_fusion.1 = (f32[350]{0:T(512)S(1)}, f32[350]{0:T(512)S(1)}, f32[350,256]{1,0:T(8,128)S(1)}) fusion(f32[30,256]{1,0:T(8,128)S(1)} %slice.619, f32[320,256]{1,0:T(8,128)S(1)} %convert_multiply_fusion.1, f32[256]{0:T(256)S(1)} %bitcast.104, f32[380,256]{1,0:T(8,128)S(1)} %pad_maximum_fusion.5, f32[256]{0:T(256)S(1)} %bitcast.106, ...), kind=kLoop, calls=%fused_computation.141 | loop fusion | flops 6002500 | bytes 11176688 | tf_op jit(solution)/shard_map/reduce_sum | solution.py:128
  18.0 6.6 %all-reduce.1 = (f32[350]{0:T(512)S(1)}, f32[350]{0:T(512)S(1)}) all-reduce(f32[350]{0:T(512)S(1)} %get-tuple-element.66, f32[350]{0:T(512)S(1)} %get-tuple-element.65), channel_id=1, replica_groups=mesh['sp'=8,'dp'=4] {'dp'}, use_global_device_ids=true, to_apply=%region_3.0 | all-reduce | flops 700 | bytes 5600 | tf_op jit(solution)/shard_map/psum | solution.py:128
  24.5 0.9 add_divide_fusion
  25.5 2.5 %fusion = bf16[256,1024]{1,0:T(8,128)(2,1)} fusion(bf16[320,256]{1,0:T(8,128)(2,1)S(1)} %fusion.177, bf16[320,256]{1,0:T(8,128)(2,1)} %get-tuple-element.147, bf16[320,256]{1,0:T(8,128)(2,1)} %get-tuple-element.149, bf16[320,256]{1,0:T(8,128)(2,1)} %get-tuple-element.148, bf16[320,256]{1,0:T(8,128)(2,1)} %get-tuple-element.150), kind=kOutput, calls=%fused_computation.43 | convolution fusion | flops 170917888 | bytes 1343488 | tf_op jit(solution)/shard_map/dot_general | solution.py:13
  28.0 2.4 %collective-permute-start.5 = (bf16[256,1024]{1,0:T(8,128)(2,1)}, bf16[256,1024]{1,0:T(8,128)(2,1)}, u32[]{:S(2)}, u32[]{:S(2)}) collective-permute-start(bf16[256,1024]{1,0:T(8,128)(2,1)} %fusion), channel_id=1, source_target_pairs={{0,4},{4,0},{8,12},{12,8},{16,20},{20,16},{24,28},{28,24},{1,5},{5... | collective-permute-start | bytes 1572872 | tf_op jit(solution)/shard_map/ppermute | solution.py:41
  30.4 0.7 slice.649
  31.5 6.4 %all-reduce = (f32[350]{0:T(512)S(1)}, f32[350]{0:T(512)S(1)}) all-reduce(f32[350]{0:T(512)S(1)} %get-tuple-element.18, f32[350]{0:T(512)S(1)} %get-tuple-element.17), channel_id=1, replica_groups=mesh['sp'=8,'dp'=4] {'dp'}, use_global_device_ids=true, to_apply=%region_7.8 | all-reduce | flops 700 | bytes 5600 | tf_op jit(solution)/shard_map/psum | solution.py:144
  37.9 0.9 subtract_multiply_fusion
  38.8 2.4 %fusion.55 = (bf16[320,256]{1,0:T(8,128)(2,1)S(1)}, f32[320,256]{1,0:T(8,128)S(1)}) fusion(bf16[320,256]{1,0:T(8,128)(2,1)} %copy-done.5, bf16[320,256]{1,0:T(8,128)(2,1)} %copy-done.3, f32[350,256]{1,0:T(8,128)S(1)} %subtract_multiply_fusion, f32[256]{0:T(256)} %bitcast.105, f32[256]{0:T(256)} %bitcast.107, f32[256]{0:T(256)} %bitcast.111, ...), kind=kLoop, calls=%fused_computation.144 | loop fusion | flops 5816320 | bytes 11009024 | tf_op jit(solution)/shard_map/convert_element_type | solution.py:153
  41.8 1.3 %fusion.2 = bf16[1024,256]{1,0:T(8,128)(2,1)} fusion(bf16[320,256]{1,0:T(8,128)(2,1)S(1)} %get-tuple-element.20, bf16[320,256]{1,0:T(8,128)(2,1)S(1)} %copy-done.20, bf16[320,256]{1,0:T(8,128)(2,1)S(1)} %copy-done.18, bf16[320,256]{1,0:T(8,128)(2,1)S(1)} %copy-done.19, bf16[320,256]{1,0:T(8,128)(2,1)S(1)} %copy-done.17), kind=kOutput, calls=%fused_computation.45 | convolution fusion | flops 170917888 | bytes 1343488 | tf_op jit(solution)/shard_map/dot_general | solution.py:13
  44.3 0.5 convolution_add_fusion
  44.9 0.9 dynamic-slice_convert_fusion
  45.8 1.4 %collective-permute-start.10 = (bf16[1024,256]{1,0:T(8,128)(2,1)}, bf16[1024,256]{1,0:T(8,128)(2,1)}, u32[]{:S(2)}, u32[]{:S(2)}) collective-permute-start(bf16[1024,256]{1,0:T(8,128)(2,1)} %fusion.2), channel_id=1, source_target_pairs={{0,4},{4,0},{8,12},{12,8},{16,20},{20,16},{24,28},{28,24},{1,5},{5... | collective-permute-start | bytes 1572872 | tf_op jit(solution)/shard_map/ppermute | solution.py:41
  47.3 1.5 %convert_add_fusion.2 = f32[256,1024]{1,0:T(8,128)S(1)} fusion(bf16[256,1024]{1,0:T(8,128)(2,1)} %collective-permute-done.5, bf16[320,256]{1,0:T(8,128)(2,1)S(1)} %copy-done.30, bf16[320,256]{1,0:T(8,128)(2,1)S(1)} %get-tuple-element.83, bf16[320,256]{1,0:T(8,128)(2,1)S(1)} %get-tuple-element.84, bf16[320,256]{1,0:T(8,128)(2,1)S(1)} %get-tuple-element.85, ...), kind=kOutput, calls=%fused_computation.50 | convolution fusion | flops 171180032 | bytes 2392064 | tf_op jit(solution)/shard_map/dot_general | solution.py:13
  48.9 0.8 dynamic-slice_convert_fusion.7
  49.6 3.6 %collective-permute-start.16 = (bf16[256,256]{1,0:T(8,128)(2,1)}, bf16[256,256]{1,0:T(8,128)(2,1)}, u32[]{:S(2)}, u32[]{:S(2)}) collective-permute-start(bf16[256,256]{1,0:T(8,128)(2,1)} %get-tuple-element.102), channel_id=1, source_target_pairs={{0,24},{4,28},{8,0},{12,4},{16,8},{20,12},{24,16},{28,20},{1,25},{... | collective-permute-start | bytes 393224 | tf_op jit(solution)/shard_map/ppermute | solution.py:59
  54.5 3.4 %collective-permute-done.6 = bf16[1024,256]{1,0:T(8,128)(2,1)S(1)} collective-permute-done((bf16[1024,256]{1,0:T(8,128)(2,1)S(1)}, bf16[1024,256]{1,0:T(8,128)(2,1)S(1)}, u32[]{:S(2)}, u32[]{:S(2)}) %collective-permute-start.6) | collective-permute-done | bytes 524320 | tf_op jit(solution)/shard_map/ppermute | solution.py:41
  58.4 0.8 dynamic-slice_convert_fusion.6
  59.2 3.2 %collective-permute-start.9 = (bf16[256,256]{1,0:T(8,128)(2,1)}, bf16[256,256]{1,0:T(8,128)(2,1)}, u32[]{:S(2)}, u32[]{:S(2)}) collective-permute-start(bf16[256,256]{1,0:T(8,128)(2,1)} %get-tuple-element.100), channel_id=1, source_target_pairs={{0,24},{4,28},{8,0},{12,4},{16,8},{20,12},{24,16},{28,20},{1,25},{... | collective-permute-start | bytes 393224 | tf_op jit(solution)/shard_map/ppermute | solution.py:59
  63.1 3.0 %collective-permute-start.17 = (f32[34,256]{1,0:T(8,128)S(1)}, f32[34,256]{1,0:T(8,128)S(1)}, u32[]{:S(2)}, u32[]{:S(2)}) collective-permute-start(f32[34,256]{1,0:T(8,128)S(1)} %broadcast_multiply_fusion), channel_id=1, source_target_pairs={{0,16},{4,20},{8,24},{12,28},{16,0},{20,4},{24,8},{28,12},{1,17},{... | collective-permute-start | bytes 104456 | tf_op jit(solution)/shard_map/ppermute | solution.py:20
  66.1 1.7 %add_convert_fusion.1 = bf16[320,1024]{1,0:T(8,128)(2,1)S(1)} fusion(bf16[320,1024]{1,0:T(8,128)(2,1)} %collective-permute-done.2, f32[320,2048]{1,0:T(8,128)} %copy-done.1, s32[]{:T(128)S(6)} %select_n.120), kind=kLoop, calls=%fused_computation.41 | loop fusion | flops 983040 | bytes 2621444 | tf_op jit(solution)/shard_map/convert_element_type | solution.py:81
  67.8 2.7 %collective-permute-done.17 = f32[34,256]{1,0:T(8,128)S(1)} collective-permute-done((f32[34,256]{1,0:T(8,128)S(1)}, f32[34,256]{1,0:T(8,128)S(1)}, u32[]{:S(2)}, u32[]{:S(2)}) %collective-permute-start.17) | collective-permute-done | bytes 34848 | tf_op jit(solution)/shard_map/ppermute | solution.py:20
  70.5 1.9 %collective-permute-start.3 = (bf16[320,1024]{1,0:T(8,128)(2,1)S(1)}, bf16[320,1024]{1,0:T(8,128)(2,1)S(1)}, u32[]{:S(2)}, u32[]{:S(2)}) collective-permute-start(bf16[320,1024]{1,0:T(8,128)(2,1)S(1)} %add_convert_fusion.1), channel_id=1, source_target_pairs={{0,2},{1,3},{2,0},{3,1},{4,6},{5,7},{6,4},{7,5},{8,10},{9,11},{10,... | collective-permute-start | bytes 1966088 | tf_op jit(solution)/shard_map/ppermute | solution.py:82
  72.6 1.5 %convert_add_fusion = f32[1024,256]{1,0:T(8,128)S(1)} fusion(bf16[1024,256]{1,0:T(8,128)(2,1)} %collective-permute-done.10, bf16[320,256]{1,0:T(8,128)(2,1)S(1)} %copy-done.15, bf16[320,256]{1,0:T(8,128)(2,1)S(1)} %copy-done.24, bf16[320,256]{1,0:T(8,128)(2,1)S(1)} %copy-done.26, bf16[320,256]{1,0:T(8,128)(2,1)S(1)} %copy-done.28, ...), kind=kOutput, calls=%fused_computation.48 | convolution fusion | flops 171180032 | bytes 2392064 | tf_op jit(solution)/shard_map/dot_general | solution.py:13
  74.1 2.4 %collective-permute-done.18 = f32[34,256]{1,0:T(8,128)S(1)} collective-permute-done((f32[34,256]{1,0:T(8,128)S(1)}, f32[34,256]{1,0:T(8,128)S(1)}, u32[]{:S(2)}, u32[]{:S(2)}) %collective-permute-start.18) | collective-permute-done | bytes 34848 | tf_op jit(solution)/shard_map/ppermute | solution.py:20
  76.6 1.4 %collective-permute-start.19 = (f32[34,256]{1,0:T(8,128)S(1)}, f32[34,256]{1,0:T(8,128)S(1)}, u32[]{:S(2)}, u32[]{:S(2)}) collective-permute-start(f32[34,256]{1,0:T(8,128)S(1)} %add.510), channel_id=1, source_target_pairs={{0,4},{4,0},{8,12},{12,8},{16,20},{20,16},{24,28},{28,24},{1,5},{5... | collective-permute-start | bytes 104456 | tf_op jit(solution)/shard_map/ppermute | solution.py:20
  78.0 2.6 %collective-permute-done.19 = f32[34,256]{1,0:T(8,128)S(1)} collective-permute-done((f32[34,256]{1,0:T(8,128)S(1)}, f32[34,256]{1,0:T(8,128)S(1)}, u32[]{:S(2)}, u32[]{:S(2)}) %collective-permute-start.19) | collective-permute-done | bytes 34848 | tf_op jit(solution)/shard_map/ppermute | solution.py:20
  80.6 0.6 slice.746
  81.2 0.6 fusion.190
  81.8 4.3 %collective-permute-done.3 = bf16[320,1024]{1,0:T(8,128)(2,1)S(1)} collective-permute-done((bf16[320,1024]{1,0:T(8,128)(2,1)S(1)}, bf16[320,1024]{1,0:T(8,128)(2,1)S(1)}, u32[]{:S(2)}, u32[]{:S(2)}) %collective-permute-start.3) | collective-permute-done | bytes 655392 | tf_op jit(solution)/shard_map/ppermute | solution.py:82
  86.1 3.5 %collective-permute-start.13 = (bf16[256,256]{1,0:T(8,128)(2,1)S(1)}, bf16[256,256]{1,0:T(8,128)(2,1)S(1)}, u32[]{:S(2)}, u32[]{:S(2)}) collective-permute-start(bf16[256,256]{1,0:T(8,128)(2,1)S(1)} %get-tuple-element.97), channel_id=1, source_target_pairs={{0,24},{4,28},{8,0},{12,4},{16,8},{20,12},{24,16},{28,20},{1,25},{... | collective-permute-start | bytes 393224 | tf_op jit(solution)/shard_map/ppermute | solution.py:59
  90.0 0.5 collective-permute-start.11
  90.5 1.7 %convert_add_fusion.5 = f32[256,256]{1,0:T(8,128)} fusion(bf16[256,256]{1,0:T(8,128)(2,1)} %collective-permute-done.9, bf16[256,256]{1,0:T(8,128)(2,1)} %collective-permute-done.8, bf16[256,256]{1,0:T(8,128)(2,1)S(1)} %collective-permute-done.7, f32[1024,256]{1,0:T(8,128)S(1)} %convert_add_fusion.1, s32[]{:T(128)S(6)} %select_n.135), kind=kLoop, calls=%fused_computation.310 | loop fusion | flops 393216 | bytes 917508 | tf_op jit(solution)/shard_map/add | solution.py:61
  92.2 1.3 %collective-permute-done.13 = bf16[256,256]{1,0:T(8,128)(2,1)S(1)} collective-permute-done((bf16[256,256]{1,0:T(8,128)(2,1)S(1)}, bf16[256,256]{1,0:T(8,128)(2,1)S(1)}, u32[]{:S(2)}, u32[]{:S(2)}) %collective-permute-start.13) | collective-permute-done | bytes 131104 | tf_op jit(solution)/shard_map/ppermute | solution.py:59
  93.5 1.2 %collective-permute-start.15 = (bf16[256,256]{1,0:T(8,128)(2,1)S(1)}, bf16[256,256]{1,0:T(8,128)(2,1)S(1)}, u32[]{:S(2)}, u32[]{:S(2)}) collective-permute-start(bf16[256,256]{1,0:T(8,128)(2,1)S(1)} %copy-done.32), channel_id=1, source_target_pairs={{0,16},{4,20},{8,24},{12,28},{16,0},{20,4},{24,8},{28,12},{1,17},{... | collective-permute-start | bytes 393224 | tf_op jit(solution)/shard_map/ppermute | solution.py:59
  94.7 8.8 %collective-permute-done.12 = bf16[256,256]{1,0:T(8,128)(2,1)S(1)} collective-permute-done((bf16[256,256]{1,0:T(8,128)(2,1)S(1)}, bf16[256,256]{1,0:T(8,128)(2,1)S(1)}, u32[]{:S(2)}, u32[]{:S(2)}) %collective-permute-start.12) | collective-permute-done | bytes 131104 | tf_op jit(solution)/shard_map/ppermute | solution.py:59
  103.5 0.8 convert_add_fusion.4
  104.3 1.1 collective-permute-done.15
  105.4 4.9 %collective-permute-done.14 = bf16[256,256]{1,0:T(8,128)(2,1)S(1)} collective-permute-done((bf16[256,256]{1,0:T(8,128)(2,1)S(1)}, bf16[256,256]{1,0:T(8,128)(2,1)S(1)}, u32[]{:S(2)}, u32[]{:S(2)}) %collective-permute-start.14) | collective-permute-done | bytes 131104 | tf_op jit(solution)/shard_map/ppermute | solution.py:59
  110.3 1.8 %convert_add_fusion.3 = f32[256,256]{1,0:T(8,128)} fusion(bf16[256,256]{1,0:T(8,128)(2,1)} %collective-permute-done.16, bf16[256,256]{1,0:T(8,128)(2,1)S(1)} %collective-permute-done.15, bf16[256,256]{1,0:T(8,128)(2,1)S(1)} %collective-permute-done.14, f32[256,1024]{1,0:T(8,128)} %copy-done.16, s32[]{:T(128)S(6)} %select_n.135), kind=kLoop, calls=%fused_computation.305 | loop fusion | flops 393216 | bytes 917508 | tf_op jit(solution)/shard_map/add | solution.py:61
  112.1 1.2 %pad_maximum_fusion.2 = bf16[320,2048]{1,0:T(8,128)(2,1)} fusion(bf16[320,1024]{1,0:T(8,128)(2,1)S(1)} %get-tuple-element.87, bf16[320,1024]{1,0:T(8,128)(2,1)S(1)} %get-tuple-element.86), kind=kLoop, calls=%fused_computation.39 | loop fusion | flops 2621440 | bytes 2621440 | tf_op jit(solution)/shard_map/concatenate | solution.py:89
  (178 shorter events, 7.0 us)
Async XLA Ops:
  0.6 3.0 %copy-start.9 = (bf16[320,2048]{1,0:T(8,128)(2,1)S(1)}, bf16[320,2048]{1,0:T(8,128)(2,1)}, u32[]{:S(2)}) copy-start(bf16[320,2048]{1,0:T(8,128)(2,1)} %param.9) | copy-start | bytes 3932164
  0.7 3.0 %copy-start.11 = (bf16[2048,256]{1,0:T(8,128)(2,1)S(1)}, bf16[2048,256]{1,0:T(8,128)(2,1)}, u32[]{:S(2)}) copy-start(bf16[2048,256]{1,0:T(8,128)(2,1)} %param.12) | copy-start | bytes 3145732
  5.4 8.1 %copy-start.35 = (f32[31,256]{1,0:T(8,128)S(1)}, f32[31,256]{1,0:T(8,128)}, u32[]{:S(2)}) copy-start(f32[31,256]{1,0:T(8,128)} %param.14) | copy-start | bytes 95236
  6.7 9.4 %collective-permute-start.1 = (f32[45,256]{1,0:T(8,128)S(1)}, f32[45,256]{1,0:T(8,128)S(1)}, u32[]{:S(2)}, u32[]{:S(2)}) collective-permute-start(f32[45,256]{1,0:T(8,128)S(1)} %pad_maximum_fusion.11), channel_id=1, source_target_pairs={{4,0},{8,4},{12,8},{16,12},{20,16},{24,20},{28,24},{5,1},{9,5},{13... | collective-permute-start | bytes 138248 | tf_op jit(solution)/shard_map/ppermute | solution.py:122
  8.0 8.1 %collective-permute-start = (f32[45,256]{1,0:T(8,128)S(1)}, f32[45,256]{1,0:T(8,128)S(1)}, u32[]{:S(2)}, u32[]{:S(2)}) collective-permute-start(f32[45,256]{1,0:T(8,128)S(1)} %pad_maximum_fusion.10), channel_id=1, source_target_pairs={{0,4},{4,8},{8,12},{12,16},{16,20},{20,24},{24,28},{1,5},{5,9},{9,... | collective-permute-start | bytes 138248 | tf_op jit(solution)/shard_map/ppermute | solution.py:121
  13.5 2.6 %copy-start.36 = (f32[1,256]{1,0:T(1,128)}, f32[1,256]{1,0:T(1,128)S(1)}, u32[]{:S(2)}) copy-start(f32[1,256]{1,0:T(1,128)S(1)} %get-tuple-element.140) | copy-start | bytes 3076
  13.5 2.6 %copy-start.37 = (f32[1,256]{1,0:T(1,128)}, f32[1,256]{1,0:T(1,128)S(1)}, u32[]{:S(2)}) copy-start(f32[1,256]{1,0:T(1,128)S(1)} %get-tuple-element.141) | copy-start | bytes 3076
  13.6 2.6 %copy-start.38 = (f32[1,256]{1,0:T(1,128)}, f32[1,256]{1,0:T(1,128)S(1)}, u32[]{:S(2)}) copy-start(f32[1,256]{1,0:T(1,128)S(1)} %get-tuple-element.142) | copy-start | bytes 3076
  13.6 2.6 %copy-start.39 = (f32[1,256]{1,0:T(1,128)}, f32[1,256]{1,0:T(1,128)S(1)}, u32[]{:S(2)}) copy-start(f32[1,256]{1,0:T(1,128)S(1)} %get-tuple-element.143) | copy-start | bytes 3076
  13.6 2.6 %copy-start.40 = (f32[1,256]{1,0:T(1,128)}, f32[1,256]{1,0:T(1,128)S(1)}, u32[]{:S(2)}) copy-start(f32[1,256]{1,0:T(1,128)S(1)} %get-tuple-element.144) | copy-start | bytes 3076
  13.6 2.6 %copy-start.41 = (f32[1,256]{1,0:T(1,128)}, f32[1,256]{1,0:T(1,128)S(1)}, u32[]{:S(2)}) copy-start(f32[1,256]{1,0:T(1,128)S(1)} %get-tuple-element.114) | copy-start | bytes 3076
  13.6 2.6 %copy-start.42 = (f32[1,256]{1,0:T(1,128)}, f32[1,256]{1,0:T(1,128)S(1)}, u32[]{:S(2)}) copy-start(f32[1,256]{1,0:T(1,128)S(1)} %get-tuple-element.115) | copy-start | bytes 3076
  25.5 5.6 %copy-start.8 = (f32[320,256]{1,0:T(8,128)S(1)}, f32[320,256]{1,0:T(8,128)}, u32[]{:S(2)}) copy-start(f32[320,256]{1,0:T(8,128)} %copy-done.7) | copy-start | bytes 983044
  25.5 5.6 %copy-start.60 = (f32[256]{0:T(256)S(1)}, f32[256]{0:T(256)}, u32[]{:S(2)}) copy-start(f32[256]{0:T(256)} %param.16) | copy-start | bytes 3076
  28.0 19.3 %collective-permute-start.5 = (bf16[256,1024]{1,0:T(8,128)(2,1)}, bf16[256,1024]{1,0:T(8,128)(2,1)}, u32[]{:S(2)}, u32[]{:S(2)}) collective-permute-start(bf16[256,1024]{1,0:T(8,128)(2,1)} %fusion), channel_id=1, source_target_pairs={{0,4},{4,0},{8,12},{12,8},{16,20},{20,16},{24,28},{28,24},{1,5},{5... | collective-permute-start | bytes 1572872 | tf_op jit(solution)/shard_map/ppermute | solution.py:41
  41.2 2.7 %copy-start.14 = (bf16[320,256]{1,0:T(8,128)(2,1)}, bf16[320,256]{1,0:T(8,128)(2,1)S(1)}, u32[]{:S(2)}) copy-start(bf16[320,256]{1,0:T(8,128)(2,1)S(1)} %get-tuple-element.20) | copy-start | bytes 491524
  43.1 14.8 %collective-permute-start.6 = (bf16[1024,256]{1,0:T(8,128)(2,1)S(1)}, bf16[1024,256]{1,0:T(8,128)(2,1)S(1)}, u32[]{:S(2)}, u32[]{:S(2)}) collective-permute-start(bf16[1024,256]{1,0:T(8,128)(2,1)S(1)} %fusion.1), channel_id=1, source_target_pairs={{0,4},{4,0},{8,12},{12,8},{16,20},{20,16},{24,28},{28,24},{1,5},{5... | collective-permute-start | bytes 1572872 | tf_op jit(solution)/shard_map/ppermute | solution.py:41
  45.8 17.3 %collective-permute-start.2 = (bf16[320,1024]{1,0:T(8,128)(2,1)}, bf16[320,1024]{1,0:T(8,128)(2,1)}, u32[]{:S(2)}, u32[]{:S(2)}) collective-permute-start(bf16[320,1024]{1,0:T(8,128)(2,1)} %dynamic-slice_convert_fusion), channel_id=1, source_target_pairs={{0,1},{1,0},{2,3},{3,2},{4,5},{5,4},{6,7},{7,6},{8,9},{9,8},{10,11... | collective-permute-start | bytes 1966088 | tf_op jit(solution)/shard_map/ppermute | solution.py:77
  45.8 26.6 %collective-permute-start.10 = (bf16[1024,256]{1,0:T(8,128)(2,1)}, bf16[1024,256]{1,0:T(8,128)(2,1)}, u32[]{:S(2)}, u32[]{:S(2)}) collective-permute-start(bf16[1024,256]{1,0:T(8,128)(2,1)} %fusion.2), channel_id=1, source_target_pairs={{0,4},{4,0},{8,12},{12,8},{16,20},{20,16},{24,28},{28,24},{1,5},{5... | collective-permute-start | bytes 1572872 | tf_op jit(solution)/shard_map/ppermute | solution.py:41
  48.8 5.1 %copy-start.16 = (f32[256,1024]{1,0:T(8,128)}, f32[256,1024]{1,0:T(8,128)S(1)}, u32[]{:S(2)}) copy-start(f32[256,1024]{1,0:T(8,128)S(1)} %convert_add_fusion.2) | copy-start | bytes 3145732
  48.9 4.9 %copy-start.10 = (bf16[320,2048]{1,0:T(8,128)(2,1)S(1)}, bf16[320,2048]{1,0:T(8,128)(2,1)}, u32[]{:S(2)}) copy-start(bf16[320,2048]{1,0:T(8,128)(2,1)} %param.9) | copy-start | bytes 3932164
  49.6 54.6 %collective-permute-start.16 = (bf16[256,256]{1,0:T(8,128)(2,1)}, bf16[256,256]{1,0:T(8,128)(2,1)}, u32[]{:S(2)}, u32[]{:S(2)}) collective-permute-start(bf16[256,256]{1,0:T(8,128)(2,1)} %get-tuple-element.102), channel_id=1, source_target_pairs={{0,24},{4,28},{8,0},{12,4},{16,8},{20,12},{24,16},{28,20},{1,25},{... | collective-permute-start | bytes 393224 | tf_op jit(solution)/shard_map/ppermute | solution.py:59
  53.9 4.5 %copy-start.21 = (bf16[320,256]{1,0:T(8,128)(2,1)}, bf16[320,256]{1,0:T(8,128)(2,1)S(1)}, u32[]{:S(2)}) copy-start(bf16[320,256]{1,0:T(8,128)(2,1)S(1)} %get-tuple-element.78) | copy-start | bytes 491524
  53.9 4.5 %copy-start.23 = (bf16[320,256]{1,0:T(8,128)(2,1)}, bf16[320,256]{1,0:T(8,128)(2,1)S(1)}, u32[]{:S(2)}) copy-start(bf16[320,256]{1,0:T(8,128)(2,1)S(1)} %get-tuple-element.79) | copy-start | bytes 491524
  53.9 4.5 %copy-start.25 = (bf16[320,256]{1,0:T(8,128)(2,1)}, bf16[320,256]{1,0:T(8,128)(2,1)S(1)}, u32[]{:S(2)}) copy-start(bf16[320,256]{1,0:T(8,128)(2,1)S(1)} %get-tuple-element.80) | copy-start | bytes 491524
  54.0 4.5 %copy-start.27 = (bf16[320,256]{1,0:T(8,128)(2,1)}, bf16[320,256]{1,0:T(8,128)(2,1)S(1)}, u32[]{:S(2)}) copy-start(bf16[320,256]{1,0:T(8,128)(2,1)S(1)} %get-tuple-element.81) | copy-start | bytes 491524
  58.4 4.1 %copy-start.6 = (bf16[320,256]{1,0:T(8,128)(2,1)S(1)}, bf16[320,256]{1,0:T(8,128)(2,1)}, u32[]{:S(2)}) copy-start(bf16[320,256]{1,0:T(8,128)(2,1)} %copy-done.5) | copy-start | bytes 491524
  59.2 30.6 %collective-permute-start.9 = (bf16[256,256]{1,0:T(8,128)(2,1)}, bf16[256,256]{1,0:T(8,128)(2,1)}, u32[]{:S(2)}, u32[]{:S(2)}) collective-permute-start(bf16[256,256]{1,0:T(8,128)(2,1)} %get-tuple-element.100), channel_id=1, source_target_pairs={{0,24},{4,28},{8,0},{12,4},{16,8},{20,12},{24,16},{28,20},{1,25},{... | collective-permute-start | bytes 393224 | tf_op jit(solution)/shard_map/ppermute | solution.py:59
  62.4 27.5 %collective-permute-start.8 = (bf16[256,256]{1,0:T(8,128)(2,1)}, bf16[256,256]{1,0:T(8,128)(2,1)}, u32[]{:S(2)}, u32[]{:S(2)}) collective-permute-start(bf16[256,256]{1,0:T(8,128)(2,1)} %get-tuple-element.101), channel_id=1, source_target_pairs={{0,16},{4,20},{8,24},{12,28},{16,0},{20,4},{24,8},{28,12},{1,17},{... | collective-permute-start | bytes 393224 | tf_op jit(solution)/shard_map/ppermute | solution.py:59
  63.1 9.5 %copy-start.15 = (bf16[320,256]{1,0:T(8,128)(2,1)S(1)}, bf16[320,256]{1,0:T(8,128)(2,1)}, u32[]{:S(2)}) copy-start(bf16[320,256]{1,0:T(8,128)(2,1)} %copy-done.14) | copy-start | bytes 491524
  63.1 9.5 %copy-start.22 = (bf16[320,256]{1,0:T(8,128)(2,1)S(1)}, bf16[320,256]{1,0:T(8,128)(2,1)}, u32[]{:S(2)}) copy-start(bf16[320,256]{1,0:T(8,128)(2,1)} %copy-done.21) | copy-start | bytes 491524
  63.1 9.5 %copy-start.24 = (bf16[320,256]{1,0:T(8,128)(2,1)S(1)}, bf16[320,256]{1,0:T(8,128)(2,1)}, u32[]{:S(2)}) copy-start(bf16[320,256]{1,0:T(8,128)(2,1)} %copy-done.23) | copy-start | bytes 491524
  63.1 9.5 %copy-start.26 = (bf16[320,256]{1,0:T(8,128)(2,1)S(1)}, bf16[320,256]{1,0:T(8,128)(2,1)}, u32[]{:S(2)}) copy-start(bf16[320,256]{1,0:T(8,128)(2,1)} %copy-done.25) | copy-start | bytes 491524
  63.1 9.5 %copy-start.28 = (bf16[320,256]{1,0:T(8,128)(2,1)S(1)}, bf16[320,256]{1,0:T(8,128)(2,1)}, u32[]{:S(2)}) copy-start(bf16[320,256]{1,0:T(8,128)(2,1)} %copy-done.27) | copy-start | bytes 491524
  63.1 7.4 %collective-permute-start.17 = (f32[34,256]{1,0:T(8,128)S(1)}, f32[34,256]{1,0:T(8,128)S(1)}, u32[]{:S(2)}, u32[]{:S(2)}) collective-permute-start(f32[34,256]{1,0:T(8,128)S(1)} %broadcast_multiply_fusion), channel_id=1, source_target_pairs={{0,16},{4,20},{8,24},{12,28},{16,0},{20,4},{24,8},{28,12},{1,17},{... | collective-permute-start | bytes 104456 | tf_op jit(solution)/shard_map/ppermute | solution.py:20
  70.5 15.6 %collective-permute-start.3 = (bf16[320,1024]{1,0:T(8,128)(2,1)S(1)}, bf16[320,1024]{1,0:T(8,128)(2,1)S(1)}, u32[]{:S(2)}, u32[]{:S(2)}) collective-permute-start(bf16[320,1024]{1,0:T(8,128)(2,1)S(1)} %add_convert_fusion.1), channel_id=1, source_target_pairs={{0,2},{1,3},{2,0},{3,1},{4,6},{5,7},{6,4},{7,5},{8,10},{9,11},{10,... | collective-permute-start | bytes 1966088 | tf_op jit(solution)/shard_map/ppermute | solution.py:82
  72.5 8.1 %copy-start.33 = (bf16[256,256]{1,0:T(8,128)(2,1)S(1)}, bf16[256,256]{1,0:T(8,128)(2,1)}, u32[]{:S(2)}) copy-start(bf16[256,256]{1,0:T(8,128)(2,1)} %get-tuple-element.99) | copy-start | bytes 393220
  72.5 4.1 %collective-permute-start.18 = (f32[34,256]{1,0:T(8,128)S(1)}, f32[34,256]{1,0:T(8,128)S(1)}, u32[]{:S(2)}, u32[]{:S(2)}) collective-permute-start(f32[34,256]{1,0:T(8,128)S(1)} %fusion.184), channel_id=1, source_target_pairs={{0,8},{4,12},{8,0},{12,4},{16,24},{20,28},{24,16},{28,20},{1,9},{5... | collective-permute-start | bytes 104456 | tf_op jit(solution)/shard_map/ppermute | solution.py:20
  76.6 4.0 %collective-permute-start.19 = (f32[34,256]{1,0:T(8,128)S(1)}, f32[34,256]{1,0:T(8,128)S(1)}, u32[]{:S(2)}, u32[]{:S(2)}) collective-permute-start(f32[34,256]{1,0:T(8,128)S(1)} %add.510), channel_id=1, source_target_pairs={{0,4},{4,0},{8,12},{12,8},{16,20},{20,16},{24,28},{28,24},{1,5},{5... | collective-permute-start | bytes 104456 | tf_op jit(solution)/shard_map/ppermute | solution.py:20
  80.6 9.9 %collective-permute-start.7 = (bf16[256,256]{1,0:T(8,128)(2,1)S(1)}, bf16[256,256]{1,0:T(8,128)(2,1)S(1)}, u32[]{:S(2)}, u32[]{:S(2)}) collective-permute-start(bf16[256,256]{1,0:T(8,128)(2,1)S(1)} %copy-done.33), channel_id=1, source_target_pairs={{0,8},{4,12},{8,16},{12,20},{16,24},{20,28},{24,0},{28,4},{1,9},{5... | collective-permute-start | bytes 393224 | tf_op jit(solution)/shard_map/ppermute | solution.py:59
  86.1 7.4 %copy-start.32 = (bf16[256,256]{1,0:T(8,128)(2,1)S(1)}, bf16[256,256]{1,0:T(8,128)(2,1)}, u32[]{:S(2)}) copy-start(bf16[256,256]{1,0:T(8,128)(2,1)} %get-tuple-element.103) | copy-start | bytes 393220
  86.1 17.4 %copy-start.31 = (bf16[256,256]{1,0:T(8,128)(2,1)S(1)}, bf16[256,256]{1,0:T(8,128)(2,1)}, u32[]{:S(2)}) copy-start(bf16[256,256]{1,0:T(8,128)(2,1)} %get-tuple-element.104) | copy-start | bytes 393220
  86.1 7.4 %collective-permute-start.13 = (bf16[256,256]{1,0:T(8,128)(2,1)S(1)}, bf16[256,256]{1,0:T(8,128)(2,1)S(1)}, u32[]{:S(2)}, u32[]{:S(2)}) collective-permute-start(bf16[256,256]{1,0:T(8,128)(2,1)S(1)} %get-tuple-element.97), channel_id=1, source_target_pairs={{0,24},{4,28},{8,0},{12,4},{16,8},{20,12},{24,16},{28,20},{1,25},{... | collective-permute-start | bytes 393224 | tf_op jit(solution)/shard_map/ppermute | solution.py:59
  89.9 13.6 %collective-permute-start.12 = (bf16[256,256]{1,0:T(8,128)(2,1)S(1)}, bf16[256,256]{1,0:T(8,128)(2,1)S(1)}, u32[]{:S(2)}, u32[]{:S(2)}) collective-permute-start(bf16[256,256]{1,0:T(8,128)(2,1)S(1)} %get-tuple-element.98), channel_id=1, source_target_pairs={{0,16},{4,20},{8,24},{12,28},{16,0},{20,4},{24,8},{28,12},{1,17},{... | collective-permute-start | bytes 393224 | tf_op jit(solution)/shard_map/ppermute | solution.py:59
  90.0 13.6 %collective-permute-start.11 = (bf16[256,256]{1,0:T(8,128)(2,1)S(1)}, bf16[256,256]{1,0:T(8,128)(2,1)S(1)}, u32[]{:S(2)}, u32[]{:S(2)}) collective-permute-start(bf16[256,256]{1,0:T(8,128)(2,1)S(1)} %get-tuple-element.96), channel_id=1, source_target_pairs={{0,8},{4,12},{8,16},{12,20},{16,24},{20,28},{24,0},{28,4},{1,9},{5... | collective-permute-start | bytes 393224 | tf_op jit(solution)/shard_map/ppermute | solution.py:59
  90.5 21.5 %collective-permute-start.4 = (bf16[320,1024]{1,0:T(8,128)(2,1)S(1)}, bf16[320,1024]{1,0:T(8,128)(2,1)S(1)}, u32[]{:S(2)}, u32[]{:S(2)}) collective-permute-start(bf16[320,1024]{1,0:T(8,128)(2,1)S(1)} %add_convert_fusion), channel_id=1, source_target_pairs={{0,1},{1,0},{2,3},{3,2},{4,5},{5,4},{6,7},{7,6},{8,9},{9,8},{10,11... | collective-permute-start | bytes 1966088 | tf_op jit(solution)/shard_map/ppermute | solution.py:86
  93.5 11.9 %collective-permute-start.15 = (bf16[256,256]{1,0:T(8,128)(2,1)S(1)}, bf16[256,256]{1,0:T(8,128)(2,1)S(1)}, u32[]{:S(2)}, u32[]{:S(2)}) collective-permute-start(bf16[256,256]{1,0:T(8,128)(2,1)S(1)} %copy-done.32), channel_id=1, source_target_pairs={{0,16},{4,20},{8,24},{12,28},{16,0},{20,4},{24,8},{28,12},{1,17},{... | collective-permute-start | bytes 393224 | tf_op jit(solution)/shard_map/ppermute | solution.py:59
  103.5 6.8 %collective-permute-start.14 = (bf16[256,256]{1,0:T(8,128)(2,1)S(1)}, bf16[256,256]{1,0:T(8,128)(2,1)S(1)}, u32[]{:S(2)}, u32[]{:S(2)}) collective-permute-start(bf16[256,256]{1,0:T(8,128)(2,1)S(1)} %copy-done.31), channel_id=1, source_target_pairs={{0,8},{4,12},{8,16},{12,20},{16,24},{20,28},{24,0},{28,4},{1,9},{5... | collective-permute-start | bytes 393224 | tf_op jit(solution)/shard_map/ppermute | solution.py:59
  (34 other events, 77.4 us)
